TPU v7x, 32 devices: a whole 2x2x4 slice. The times are simulated.
32 devices in a mesh: sp: 8 (over z, y), tp: 4 (over x, core).
Axes of the slice: x: 2, y: 2, z: 4, core: 2. Of those that a mesh axis runs over, the one named last changes fastest.
Arguments:
- out_grad: bfloat16 [1024, 2048], P('sp', 'tp'), may hold values from -6 to 6
- route_ids: int32 [1024, 2], P('sp'), may hold values from 0 to 7, as said below
- route_weight: float32 [1024, 2], P('sp'), may hold values from 0.1 to 0.9
- expert_inputs: bfloat16 [8, 512, 2048], P('sp'), may hold values from -6 to 6
- gate_weight: bfloat16 [8, 2048, 3072], P('sp', None, 'tp'), may hold values from -0.125 to 0.125
- up_weight: bfloat16 [8, 2048, 3072], P('sp', None, 'tp'), may hold values from -0.125 to 0.125
- down_weight: bfloat16 [8, 3072, 2048], P('sp', 'tp'), may hold values from -0.109375 to 0.109375
- out_gate: bfloat16 [1024, 2048], P('sp', 'tp'), may hold values from -6 to 6
- in_gate: bfloat16 [1024, 2048], P('sp', 'tp'), may hold values from -6 to 6
- values: bfloat16 [1024, 2048], P('sp', 'tp'), may hold values from -6 to 6
- conv_out: bfloat16 [1024, 2048], P('sp', 'tp'), may hold values from -6 to 6
- conv_taps: bfloat16 [3, 2048], P(None, 'tp'), may hold values from -3.5 to 3.5
- proj_weight: bfloat16 [2048, 2048], P(None, 'tp'), may hold values from -0.125 to 0.125
Outputs:
- resid_grad: bfloat16 [1024, 2048], P('sp', 'tp')
- out_gate_grad: bfloat16 [1024, 2048], P('sp', 'tp')
- in_gate_grad: bfloat16 [1024, 2048], P('sp', 'tp')
- values_grad: bfloat16 [1024, 2048], P('sp', 'tp')
- proj_grad: float32 [2048, 2048], P('sp', 'tp')
- gate_grad: bfloat16 [8, 2048, 3072], P('sp', None, 'tp')
- up_grad: bfloat16 [8, 2048, 3072], P('sp', None, 'tp')
- down_grad: bfloat16 [8, 3072, 2048], P('sp', 'tp')
Inputs may be any that keep to these rules, and one draw needn't show every extreme that they name: `route_ids`: each row names two different experts. Among the rows of one device (aligned blocks of 128 rows) no expert is named more than 64 times, and in every draw one expert is named exactly 64 times in every block.
All inputs are finite; a program needn't handle non-finite values.
Results may differ from a plain program's by a relative error of at most 0.017.
Values may be sent and summed in bfloat16 or wider, within the bound.
A program may use at most 128 MiB of HBM per device.

v0:
```python
import math

import jax
import jax.numpy as jnp
from jax import lax
from jax.sharding import PartitionSpec as P


def extended(x, sides, width):
    for axis, dim in sides:
        devices, length = (lax.axis_size(axis), x.shape[dim])
        up = [(i, (i + 1) % devices) for i in range(devices - 1)]
        down = [(j, i) for i, j in up]
        last = lax.slice_in_dim(x, length - width, length, axis=dim)
        first = lax.slice_in_dim(x, 0, width, axis=dim)
        before = lax.ppermute(last, axis, up)
        after = lax.ppermute(first, axis, down)
        x = jnp.concatenate([before, x, after], axis=dim)
    return x


def contract_first(left, right):
    return lax.dot_general(
        left, right, (((0,), (0,)), ((), ())), preferred_element_type=jnp.float32
    )


def contract_last(left, right):
    return lax.dot_general(
        left, right, (((1,), (1,)), ((), ())), preferred_element_type=jnp.float32
    )


def expert_backward(inputs, routed, gate_w, up_w, down_w):
    pre_gate = jnp.dot(inputs, gate_w, preferred_element_type=jnp.float32)
    pre_up = jnp.dot(inputs, up_w, preferred_element_type=jnp.float32)
    sigmoid_g = jax.nn.sigmoid(pre_gate)
    activated = pre_gate * sigmoid_g
    hidden = (activated * pre_up).astype(jnp.bfloat16)
    d_hidden = contract_last(routed, down_w)
    d_gate = (d_hidden * pre_up * sigmoid_g * (1.0 + pre_gate * (1.0 - sigmoid_g))).astype(
        jnp.bfloat16
    )
    d_up = (d_hidden * activated).astype(jnp.bfloat16)
    partial_value = contract_last(d_gate, gate_w) + contract_last(d_up, up_w)
    grad_set = (
        contract_first(inputs, d_gate),
        contract_first(inputs, d_up),
        contract_first(hidden, routed),
    )
    return (partial_value, grad_set)


def expert_pass(outgoing, input_rows, gate_weight, up_weight, down_weight):
    arrived = lax.all_to_all(outgoing, "sp", split_axis=0, concat_axis=1, tiled=True)
    routed = lax.all_gather(arrived, "tp", axis=2, tiled=True)
    partial_value, grad_set = expert_backward(
        input_rows[0], routed[0], gate_weight[0], up_weight[0], down_weight[0]
    )
    partials = [partial_value]
    gate_list = [grad_set[0]]
    up_list = [grad_set[1]]
    down_list = [grad_set[2]]
    summed = lax.psum_scatter(
        jnp.stack(partials).astype(jnp.bfloat16), "tp", scatter_dimension=2, tiled=True
    )
    returned = lax.all_to_all(summed, "sp", split_axis=1, concat_axis=0, tiled=True)
    return (returned, (jnp.stack(gate_list), jnp.stack(up_list), jnp.stack(down_list)))


def per_device(
    out_grad,
    route_ids,
    route_weight,
    expert_inputs,
    gate_weight,
    up_weight,
    down_weight,
    out_gate,
    in_gate,
    values,
    conv_out,
    conv_taps,
    proj_weight,
):
    sp_devices = lax.axis_size("sp")
    tok_rows = out_grad.shape[0]
    local_experts = gate_weight.shape[0]
    all_experts = sp_devices * local_experts
    capacity = 4 * tok_rows // all_experts
    flat_ids = route_ids.reshape(-1)
    onehot = (flat_ids[:, None] == jnp.arange(all_experts, dtype=jnp.int32)[None, :]).astype(
        jnp.int32
    )
    ranked = jnp.sum((jnp.cumsum(onehot, axis=0) - onehot) * onehot, axis=1)
    slot_ids = flat_ids * capacity + ranked
    dispatch = (
        jnp.arange(all_experts * capacity, dtype=jnp.int32)[:, None] == slot_ids[None, :]
    ).astype(jnp.bfloat16)
    weighted = (
        (route_weight[:, :, None] * out_grad.astype(jnp.float32)[:, None, :])
        .astype(jnp.bfloat16)
        .reshape(2 * tok_rows, -1)
    )
    outgoing = jnp.dot(dispatch, weighted, preferred_element_type=jnp.float32).astype(jnp.bfloat16)
    outgoing = outgoing.reshape(all_experts, capacity, -1)
    returned, totals = expert_pass(outgoing, expert_inputs, gate_weight, up_weight, down_weight)
    slot_scale = 1.0 / math.sqrt(expert_inputs.shape[1])
    gate_grad = (totals[0] * slot_scale).astype(jnp.bfloat16)
    up_grad = (totals[1] * slot_scale).astype(jnp.bfloat16)
    down_grad = (totals[2] * slot_scale).astype(jnp.bfloat16)
    combiner = jnp.sum(dispatch.reshape(all_experts * capacity, tok_rows, 2), axis=2)
    moe_part = contract_first(combiner, returned.reshape(all_experts * capacity, -1))
    resid_grad = (out_grad.astype(jnp.float32) + moe_part).astype(jnp.bfloat16)
    resid_full = lax.all_gather(resid_grad, "tp", axis=1, tiled=True)
    mix_grad = jnp.dot(resid_full, proj_weight, preferred_element_type=jnp.float32)
    gate_vals = out_gate.astype(jnp.float32)
    conv_vals = conv_out.astype(jnp.float32)
    mixed_in = (gate_vals * conv_vals).astype(jnp.bfloat16)
    out_gate_grad = (mix_grad * conv_vals).astype(jnp.bfloat16)
    conv_grad = (mix_grad * gate_vals).astype(jnp.bfloat16)
    padded = extended(conv_grad, (("sp", 0),), 1).astype(jnp.float32)
    tap_vals = conv_taps.astype(jnp.float32)
    value_grad = padded[2:] * tap_vals[0] + padded[1:-1] * tap_vals[1] + padded[:-2] * tap_vals[2]
    in_gate_grad = (value_grad * values.astype(jnp.float32)).astype(jnp.bfloat16)
    values_grad = (value_grad * in_gate.astype(jnp.float32)).astype(jnp.bfloat16)
    token_scale = 1.0 / math.sqrt(tok_rows * sp_devices)
    columns = lax.all_to_all(resid_full, "sp", split_axis=1, concat_axis=0, tiled=True)
    proj_sum = contract_first(columns, lax.all_gather(mixed_in, "sp", axis=0, tiled=True))
    proj_grad = proj_sum * token_scale
    return (
        resid_grad,
        out_gate_grad,
        in_gate_grad,
        values_grad,
        proj_grad,
        gate_grad,
        up_grad,
        down_grad,
    )


def solution(mesh):
    in_specs = (
        P("sp", "tp"),
        P("sp", None),
        P("sp", None),
        P("sp", None, None),
        P("sp", None, "tp"),
        P("sp", None, "tp"),
        P("sp", "tp", None),
        P("sp", "tp"),
        P("sp", "tp"),
        P("sp", "tp"),
        P("sp", "tp"),
        P(None, "tp"),
        P(None, "tp"),
    )
    out_specs = (
        P("sp", "tp"),
        P("sp", "tp"),
        P("sp", "tp"),
        P("sp", "tp"),
        P("sp", "tp"),
        P("sp", None, "tp"),
        P("sp", None, "tp"),
        P("sp", "tp", None),
    )
    return jax.shard_map(
        per_device, mesh=mesh, in_specs=in_specs, out_specs=out_specs, check_vma=False
    )
```

profile of v0, /device:TPU:0, one launch (start us, length us, event | category | flops | bytes accessed | tf_op | source)
XLA Modules:
  0.0 198.5 jit_solution(15342331069827276)
XLA Ops:
  15.8 21.7 %all_to_all.40 = bf16[8,64,512]{2,1,0:T(8,128)(2,1)} all-to-all(bf16[8,64,512]{2,1,0:T(8,128)(2,1)S(1)} %bitcast.88), channel_id=1, replica_groups=mesh['sp'=8,'tp'=4] {'sp'}, dimensions={0} | all-to-all | bytes 1048576 | tf_op jit(solution)/shard_map/all_to_all | solution.py:55
  37.6 4.7 %fusion.2 = f32[512,768]{1,0:T(8,128)} fusion(bf16[1,2048,768]{2,1,0:T(8,128)(2,1)S(1)} %copy-done, bf16[1,512,2048]{2,1,0:T(8,128)(2,1)} %param.16), kind=kOutput, calls=%fused_computation.6 | convolution fusion | flops 1610612736 | bytes 6815744 | tf_op jit(solution)/shard_map/dot_general | solution.py:35
  42.3 3.0 %fusion.6 = f32[512,768]{1,0:T(8,128)} fusion(bf16[1,2048,768]{2,1,0:T(8,128)(2,1)S(1)} %copy-done.9, bf16[1,512,2048]{2,1,0:T(8,128)(2,1)S(1)} %copy-done.11), kind=kOutput, calls=%fused_computation.10 | convolution fusion | flops 1610612736 | bytes 6815744 | tf_op jit(solution)/shard_map/dot_general | solution.py:36
  45.3 14.0 %all-gather.3.cloned.1.call-done = bf16[1,512,2048]{2,1,0:T(8,128)(2,1)} async-done(((bf16[1,512,512]{2,1,0:T(8,128)(2,1)}), bf16[1,512,2048]{2,1,0:T(8,128)(2,1)}) %all-gather.3.cloned.1.call-update) | async-done | bytes 2097168 | tf_op jit(solution)/shard_map/all_gather | solution.py:56
  59.3 5.6 %multiply_convert_fusion.4 = (bf16[512,768]{1,0:T(8,128)(2,1)S(1)}, bf16[512,768]{1,0:T(8,128)(2,1)S(1)}) fusion(f32[512,768]{1,0:T(8,128)} %fusion.2, f32[512,768]{1,0:T(8,128)} %fusion.6, bf16[1,768,2048]{2,1,0:T(8,128)(2,1)} %param.19, bf16[1,512,2048]{2,1,0:T(8,128)(2,1)} %all-gather.3.cloned.1.call-done), kind=kOutput, calls=%fused_computation.25 | convolution fusion | flops 1615724544 | bytes 9961472 | tf_op jit(solution)/shard_map/dot_general | solution.py:29
  67.4 3.1 %fusion.15 = bf16[1,512,2048]{2,1,0:T(8,128)(2,1)} fusion(f32[512,2048]{1,0:T(8,128)S(1)} %fusion, bf16[512,768]{1,0:T(8,128)(2,1)S(1)} %get-tuple-element.58, bf16[1,2048,768]{2,1,0:T(8,128)(2,1)S(1)} %copy-done.10), kind=kOutput, calls=%fused_computation.17 | convolution fusion | flops 1612709888 | bytes 10223616 | tf_op jit(solution)/shard_map/dot_general | solution.py:29
  70.8 31.1 %reduce-scatter.2.cloned.1.call-done = bf16[1,512,512]{2,1,0:T(8,128)(2,1)} async-done(((bf16[1,512,2048]{2,1,0:T(8,128)(2,1)}), bf16[1,512,512]{2,1,0:T(8,128)(2,1)}) %reduce-scatter.2.cloned.1.call-update) | async-done | bytes 524304 | tf_op jit(solution)/shard_map/reduce_scatter | solution.py:64
  101.9 2.8 %copy.77 = bf16[1,512,512]{2,0,1:T(2,128)(2,1)} copy(bf16[1,512,512]{2,1,0:T(8,128)(2,1)} %reduce-scatter.2.cloned.1.call-done) | data formatting | bytes 1048576 | tf_op jit(solution)/shard_map/reduce_scatter | solution.py:64
  105.2 5.6 %reduce.3 = bf16[512,512]{1,0:T(8,128)(2,1)} reduce(bf16[512,1,512]{2,1,0:T(2,128)(2,1)} %bitcast.84, bf16[]{:T(256)} %broadcast.62), dimensions={1}, to_apply=%bitcast.82.reduce_sub_computation | reduce | bytes 1048578
  110.8 2.2 %reshape.85 = bf16[8,2,16384]{2,1,0:T(2,128)(2,1)} reshape(bf16[512,512]{1,0:T(8,128)(2,1)} %reduce.3) | data formatting | bytes 1048576
  113.0 5.5 %all-to-all-start.1 = ((bf16[8,2,16384]{2,1,0:T(2,128)(2,1)}), bf16[8,2,16384]{2,1,0:T(2,128)(2,1)}, u32[]{:S(2)}, u32[]{:S(2)}) async-start(bf16[8,2,16384]{2,1,0:T(2,128)(2,1)} %reshape.85), calls=%async_computation.2 | async-start | bytes 1048576 | tf_op jit(solution)/shard_map/all_to_all | solution.py:67
  118.9 5.4 %fusion.10 = bf16[1,2048,768]{1,2,0:T(8,128)(2,1)} fusion(bf16[512,768]{1,0:T(8,128)(2,1)} %copy-done.13, bf16[1,512,2048]{2,1,0:T(8,128)(2,1)} %param.16), kind=kOutput, calls=%fused_computation.14 | convolution fusion | flops 1613758464 | bytes 6029312 | tf_op jit(solution)/shard_map/dot_general | solution.py:23
  124.2 8.7 %all-to-all-done.1 = bf16[8,2,16384]{2,1,0:T(2,128)(2,1)} async-done(((bf16[8,2,16384]{2,1,0:T(2,128)(2,1)}), bf16[8,2,16384]{2,1,0:T(2,128)(2,1)}, u32[]{:S(2)}, u32[]{:S(2)}) %all-to-all-start.1) | async-done | bytes 524320 | tf_op jit(solution)/shard_map/all_to_all | solution.py:67
  132.9 3.5 %reshape.86 = bf16[512,1,512]{2,1,0:T(2,128)(2,1)} reshape(bf16[8,2,16384]{2,1,0:T(2,128)(2,1)} %all-to-all-done.1) | data formatting | bytes 1048576
  137.9 6.5 %all_gather.10 = bf16[128,2048]{1,0:T(8,128)(2,1)S(1)} all-gather(bf16[128,512]{1,0:T(8,128)(2,1)S(1)} %fusion.25), channel_id=1, replica_groups=mesh['sp'=8,'tp'=4] {'tp'}, dimensions={1}, use_global_device_ids=true | all-gather | bytes 655360 | tf_op jit(solution)/shard_map/all_gather | solution.py:115
  145.2 2.8 %fusion.31 = (bf16[128,512]{1,0:T(8,128)(2,1)S(1)}, bf16[128,512]{1,0:T(8,128)(2,1)}, bf16[128,512]{1,0:T(8,128)(2,1)}) fusion(bf16[128,512]{1,0:T(8,128)(2,1)} %param.20, bf16[128,512]{1,0:T(8,128)(2,1)} %param.23, bf16[128,2048]{1,0:T(8,128)(2,1)S(1)} %all_gather.10, bf16[2048,512]{1,0:T(8,128)(2,1)} %param.25), kind=kOutput, calls=%fused_computation.44 | convolution fusion | flops 268959744 | bytes 3276800 | tf_op jit(solution)/shard_map/dot_general | solution.py:116
  148.0 6.1 %fusion.12 = bf16[1,768,2048]{2,1,0:T(8,128)(2,1)} fusion(bf16[1,512,2048]{2,1,0:T(8,128)(2,1)} %all-gather.3.cloned.1.call-done, f32[512,768]{1,0:T(8,128)} %fusion.6, f32[512,768]{1,0:T(8,128)} %fusion.2), kind=kOutput, calls=%fused_computation.16 | convolution fusion | flops 1616117760 | bytes 8388608 | tf_op jit(solution)/shard_map/dot_general | solution.py:23
  154.8 3.4 %collective-permute-start = (bf16[1,512]{1,0:T(2,128)(2,1)}, bf16[1,512]{1,0:T(2,128)(2,1)S(1)}, u32[]{:S(2)}, u32[]{:S(2)}) collective-permute-start(bf16[1,512]{1,0:T(2,128)(2,1)} %get-tuple-element.63), channel_id=1, source_target_pairs={{0,4},{4,8},{8,12},{12,16},{16,20},{20,24},{24,28},{1,5},{5,9},{9,... | collective-permute-start | bytes 3080 | tf_op jit(solution)/shard_map/ppermute | solution.py:16
  160.3 5.8 %all-to-all-start.2 = ((bf16[128,8,256]{2,0,1:T(8,128)(2,1)}), bf16[128,8,256]{2,0,1:T(8,128)(2,1)}, u32[]{:S(2)}, u32[]{:S(2)}) async-start(bf16[128,8,256]{2,0,1:T(8,128)(2,1)} %bitcast.86), calls=%async_computation.3 | async-start | bytes 1048576 | tf_op jit(solution)/shard_map/all_to_all | solution.py:128
  166.0 5.3 %fusion.11 = bf16[1,2048,768]{1,2,0:T(8,128)(2,1)} fusion(bf16[512,768]{1,0:T(8,128)(2,1)} %copy-done.12, bf16[1,512,2048]{2,1,0:T(8,128)(2,1)} %param.16), kind=kOutput, calls=%fused_computation.15 | convolution fusion | flops 1613758464 | bytes 6029312 | tf_op jit(solution)/shard_map/dot_general | solution.py:23
  171.3 4.6 %copy.66 = bf16[1,2048,768]{2,1,0:T(8,128)(2,1)} copy(bf16[1,2048,768]{1,2,0:T(8,128)(2,1)} %fusion.10) | data formatting | bytes 6291456
  176.0 4.7 %copy.67 = bf16[1,2048,768]{2,1,0:T(8,128)(2,1)} copy(bf16[1,2048,768]{1,2,0:T(8,128)(2,1)} %fusion.11) | data formatting | bytes 6291456
  182.8 5.7 %all-to-all-done.2 = bf16[128,8,256]{2,0,1:T(8,128)(2,1)} async-done(((bf16[128,8,256]{2,0,1:T(8,128)(2,1)}), bf16[128,8,256]{2,0,1:T(8,128)(2,1)}, u32[]{:S(2)}, u32[]{:S(2)}) %all-to-all-start.2) | async-done | bytes 524320 | tf_op jit(solution)/shard_map/all_to_all | solution.py:128
  189.3 2.6 %convolution_multiply_fusion = f32[256,512]{1,0:T(8,128)} fusion(bf16[1024,256]{1,0:T(8,128)(2,1)} %bitcast.14, bf16[1024,512]{1,0:T(8,128)(2,1)} %all-gather.5.cloned.1.call-done), kind=kOutput, calls=%fused_computation.30 | convolution fusion | flops 268566528 | bytes 2097152 | tf_op jit(solution)/shard_map/dot_general | solution.py:23
  (66 shorter events, 20.1 us)
Async XLA Ops:
  7.2 30.4 %copy-start = (bf16[1,2048,768]{2,1,0:T(8,128)(2,1)S(1)}, bf16[1,2048,768]{2,1,0:T(8,128)(2,1)}, u32[]{:S(2)}) copy-start(bf16[1,2048,768]{2,1,0:T(8,128)(2,1)} %param.17) | copy-start | bytes 9437188
  7.2 52.1 %all-gather.3.cloned.1.call-start = ((), (), s32[]{:S(2)}) async-start(), calls=%async_computation.4 | async-start | bytes 2621440 | tf_op jit(solution)/shard_map/all_gather | solution.py:56
  37.6 64.3 %reduce-scatter.2.cloned.1.call-start = ((), (), s32[]{:S(2)}) async-start(), calls=%async_computation.5 | async-start | bytes 2621440 | tf_op jit(solution)/shard_map/reduce_scatter | solution.py:64
  37.6 4.7 %copy-start.9 = (bf16[1,2048,768]{2,1,0:T(8,128)(2,1)S(1)}, bf16[1,2048,768]{2,1,0:T(8,128)(2,1)}, u32[]{:S(2)}) copy-start(bf16[1,2048,768]{2,1,0:T(8,128)(2,1)} %param.18) | copy-start | bytes 9437188
  37.6 4.7 %copy-start.11 = (bf16[1,512,2048]{2,1,0:T(8,128)(2,1)S(1)}, bf16[1,512,2048]{2,1,0:T(8,128)(2,1)}, u32[]{:S(2)}) copy-start(bf16[1,512,2048]{2,1,0:T(8,128)(2,1)} %param.16) | copy-start | bytes 6291460
  64.9 1.9 copy-start.13
  64.9 1.9 copy-start.12
  64.9 2.5 %copy-start.10 = (bf16[1,2048,768]{2,1,0:T(8,128)(2,1)S(1)}, bf16[1,2048,768]{2,1,0:T(8,128)(2,1)}, u32[]{:S(2)}) copy-start(bf16[1,2048,768]{2,1,0:T(8,128)(2,1)} %param.18) | copy-start | bytes 9437188
  104.7 14.0 %copy-start.8 = (s32[128,2]{0,1:T(2,128)S(1)}, s32[128,2]{0,1:T(2,128)}, u32[]{:S(2)}) copy-start(s32[128,2]{0,1:T(2,128)} %param.14) | copy-start | bytes 3076
  104.7 14.1 %copy-start.7 = (bf16[3,512]{1,0:T(4,128)(2,1)S(1)}, bf16[3,512]{1,0:T(4,128)(2,1)}, u32[]{:S(2)}) copy-start(bf16[3,512]{1,0:T(4,128)(2,1)} %param.24) | copy-start | bytes 9220
  113.0 19.9 %all-to-all-start.1 = ((bf16[8,2,16384]{2,1,0:T(2,128)(2,1)}), bf16[8,2,16384]{2,1,0:T(2,128)(2,1)}, u32[]{:S(2)}, u32[]{:S(2)}) async-start(bf16[8,2,16384]{2,1,0:T(2,128)(2,1)} %reshape.85), calls=%async_computation.2 | async-start | bytes 1048576 | tf_op jit(solution)/shard_map/all_to_all | solution.py:67
  118.5 70.8 %all-gather.5.cloned.1.call-start = ((), (), s32[]{:S(2)}) async-start(), calls=%async_computation.6 | async-start | bytes 1179648 | tf_op jit(solution)/shard_map/all_gather | solution.py:129
  118.8 17.6 %copy-start.3 = (bf16[128,512]{1,0:T(8,128)(2,1)S(1)}, bf16[128,512]{1,0:T(8,128)(2,1)}, u32[]{:S(2)}) copy-start(bf16[128,512]{1,0:T(8,128)(2,1)} %param.13) | copy-start | bytes 393220
  137.9 16.3 %copy-start.4 = (bf16[128,512]{1,0:T(8,128)(2,1)}, bf16[128,512]{1,0:T(8,128)(2,1)S(1)}, u32[]{:S(2)}) copy-start(bf16[128,512]{1,0:T(8,128)(2,1)S(1)} %fusion.25) | copy-start | bytes 393220
  144.4 0.8 copy-start.1
  148.0 11.4 %copy-start.2 = (bf16[128,2048]{1,0:T(8,128)(2,1)S(1)}, bf16[128,2048]{1,0:T(8,128)(2,1)}, u32[]{:S(2)}) copy-start(bf16[128,2048]{1,0:T(8,128)(2,1)} %copy-done.1) | copy-start | bytes 1572868
  154.8 25.9 %collective-permute-start = (bf16[1,512]{1,0:T(2,128)(2,1)}, bf16[1,512]{1,0:T(2,128)(2,1)S(1)}, u32[]{:S(2)}, u32[]{:S(2)}) collective-permute-start(bf16[1,512]{1,0:T(2,128)(2,1)} %get-tuple-element.63), channel_id=1, source_target_pairs={{0,4},{4,8},{8,12},{12,16},{16,20},{20,24},{24,28},{1,5},{5,9},{9,... | collective-permute-start | bytes 3080 | tf_op jit(solution)/shard_map/ppermute | solution.py:16
  158.1 22.5 %collective-permute-start.1 = (bf16[1,512]{1,0:T(2,128)(2,1)}, bf16[1,512]{1,0:T(2,128)(2,1)}, u32[]{:S(2)}, u32[]{:S(2)}) collective-permute-start(bf16[1,512]{1,0:T(2,128)(2,1)} %get-tuple-element.64), channel_id=1, source_target_pairs={{4,0},{8,4},{12,8},{16,12},{20,16},{24,20},{28,24},{5,1},{9,5},{13... | collective-permute-start | bytes 3080 | tf_op jit(solution)/shard_map/ppermute | solution.py:17
  160.3 28.2 %all-to-all-start.2 = ((bf16[128,8,256]{2,0,1:T(8,128)(2,1)}), bf16[128,8,256]{2,0,1:T(8,128)(2,1)}, u32[]{:S(2)}, u32[]{:S(2)}) async-start(bf16[128,8,256]{2,0,1:T(8,128)(2,1)} %bitcast.86), calls=%async_computation.3 | async-start | bytes 1048576 | tf_op jit(solution)/shard_map/all_to_all | solution.py:128
  176.0 5.4 %copy-start.5 = (bf16[128,512]{1,0:T(8,128)(2,1)S(1)}, bf16[128,512]{1,0:T(8,128)(2,1)}, u32[]{:S(2)}) copy-start(bf16[128,512]{1,0:T(8,128)(2,1)} %param.21) | copy-start | bytes 393220
  176.0 6.2 %copy-start.6 = (bf16[128,512]{1,0:T(8,128)(2,1)S(1)}, bf16[128,512]{1,0:T(8,128)(2,1)}, u32[]{:S(2)}) copy-start(bf16[128,512]{1,0:T(8,128)(2,1)} %param.22) | copy-start | bytes 393220
Sparse Core Ops, SparseCore 0:
  37.7 21.5 all-gather.2
  70.7 31.1 reduce-scatter.1
  148.1 41.1 all-gather.4
where the time goes:
time: 200 us; the launch traced here: 198 us
  waiting for transfers between devices  60.4 us (30%)
  matrix products  43.4 us (22%)
  blocking collectives  28.2 us (14%)
  local copies, waits for them, and re-layouts  27.8 us (14%)
  starting transfers between devices  16.2 us (8%)
  between operations  14 us (7%)
  other arithmetic  8.51 us (4%)
    reduce_scatter x1, waiting for transfers between devices, expert_pass(): lax.psum_scatter(jnp.stack(partials).astype(jnp.bfloat16), 'tp', scatter_...  31.1 us
    all_to_all x1, blocking collectives, expert_pass(): lax.all_to_all(outgoing, 'sp', split_axis=0, concat_axis=1, tiled=True)  21.7 us
    dot_general x5, matrix products, contract_first(): lax.dot_general(left, right, (((0,), (0,)), ((), ())), preferred_element_...  20.9 us
    unnamed x35, local copies, waits for them, and re-layouts  18.7 us
    all_gather x1, waiting for transfers between devices, expert_pass(): routed = lax.all_gather(arrived, 'tp', axis=2, tiled=True)  14 us
    dot_general x3, matrix products, contract_last(): lax.dot_general(left, right, (((1,), (1,)), ((), ())), preferred_element_...  10.6 us
    all_to_all x1, waiting for transfers between devices, expert_pass(): lax.all_to_all(summed, 'sp', split_axis=1, concat_axis=0, tiled=True)  8.71 us
    all_gather x1, blocking collectives, per_device(): resid_full = lax.all_gather(resid_grad, 'tp', axis=1, tiled=True)  6.5 us
  transfers between devices with their start and end apart: 7, of which 5 were waited for; matrix products, arithmetic and copies ran while one was open for 19% of the time, Pallas kernels for 0%

commit v1 on v0

v1 whole, which is shorter than its diff:
```python
import functools
import math

import jax
import jax.numpy as jnp
from jax import lax
from jax.experimental import pallas as pl
from jax.experimental.pallas import tpu as pltpu
from jax.sharding import PartitionSpec as P

BF = jnp.bfloat16
F32 = jnp.float32
MESH = pl.DeviceIdType.MESH
VMEM = pl.BlockSpec(memory_space=pltpu.VMEM)
ANY = pl.BlockSpec(memory_space=pl.ANY)


def dot(left, right, dims):
    return lax.dot_general(left, right, ((dims[0], dims[1]), ((), ())), preferred_element_type=F32)


def remote(src, dst, send, recv, device):
    return pltpu.make_async_remote_copy(
        src_ref=src, dst_ref=dst, send_sem=send, recv_sem=recv, device_id=device, device_id_type=MESH
    )


def greet(n_sp, me, partners):
    barrier = pltpu.get_barrier_semaphore()
    for d in range(1, n_sp):
        pl.semaphore_signal(
            barrier, inc=1, device_id={"sp": lax.rem(me + d, n_sp)}, device_id_type=MESH
        )
    for tp in partners:
        pl.semaphore_signal(barrier, inc=1, device_id={"tp": tp}, device_id_type=MESH)
    pl.semaphore_wait(barrier, n_sp - 1 + len(partners))


class Exchange:
    def __init__(self, n_sp, me, tp, sib, far, src_at, dst_at, sems):
        self.n_sp, self.me, self.tp, self.sib, self.far = n_sp, me, tp, sib, far
        self.src_at, self.dst_at, self.sems = src_at, dst_at, sems

    def source(self, d):
        return lax.rem(self.me - d + self.n_sp, self.n_sp)

    def sp_copy(self, d):
        to = lax.rem(self.me + d, self.n_sp)
        return remote(
            self.src_at(to), self.dst_at(self.tp, self.me),
            self.sems.at[0, d], self.sems.at[1, d], {"sp": to},
        )

    def far_copy(self, d):
        place = self.dst_at(self.tp, self.source(d))
        return remote(place, place, self.sems.at[2, d], self.sems.at[3, d], {"tp": self.far})

    def sib_copy(self, d):
        place = self.dst_at(self.tp, self.source(d))
        return remote(place, place, self.sems.at[4, d], self.sems.at[5, d], {"tp": self.sib})

    def hand_copy(self, d):
        place = self.dst_at(self.far, self.source(d))
        return remote(place, place, self.sems.at[6, d], self.sems.at[7, d], {"tp": self.sib})

    def start(self):
        for d in range(1, self.n_sp):
            self.sp_copy(d).start()
        own = pltpu.make_async_copy(
            self.src_at(self.me), self.dst_at(self.tp, self.me), self.sems.at[0, 0]
        )
        own.start()
        own.wait()
        self.far_copy(0).start()
        self.sib_copy(0).start()

    def step(self, d):
        self.sp_copy(d).wait_recv()
        self.far_copy(d).start()
        self.sib_copy(d).start()
        self.far_copy(d - 1).wait_recv()
        self.hand_copy(d - 1).start()

    def steps(self, first, last):
        @pl.loop(first, last)
        def _(d):
            self.step(d)

    def finish(self):
        n = self.n_sp
        self.far_copy(n - 1).wait_recv()
        self.hand_copy(n - 1).start()

        @pl.loop(0, n)
        def _(d):
            self.far_copy(d).wait_send()
            self.sib_copy(d).wait_send()
            self.sib_copy(d).wait_recv()
            self.hand_copy(d).wait_send()
            self.hand_copy(d).wait_recv()

        @pl.loop(1, n)
        def _(d):
            self.sp_copy(d).wait_send()


def expert_kernel(
    n_sp, n_tp, experts,
    og_ref, ids_ref, rw_ref, x_hbm, gw_hbm, uw_hbm, dw_hbm,
    routed, hidden, dall, resid, rfull, quarter,
    x, w, dw, pre, outgoing, parts, from_sib, far_out, far_in, total, final, back, disp,
    load_sems, ex_sems, sib_sems, far_sems, ret_sems, gat_sems,
):
    me, tp = lax.axis_index("sp"), lax.axis_index("tp")
    sib = tp + 1 - 2 * lax.rem(tp, 2)
    far = lax.rem(tp + n_tp // 2, n_tp)
    tokens, chan = og_ref.shape
    slots, width = x.shape
    hid = dw.shape[0]
    cap = slots // n_sp
    local = experts // n_sp

    loads = [
        pltpu.make_async_copy(x_hbm.at[0], x, load_sems.at[0]),
        pltpu.make_async_copy(gw_hbm.at[0], w.at[:, pl.ds(0, hid)], load_sems.at[1]),
        pltpu.make_async_copy(uw_hbm.at[0], w.at[:, pl.ds(hid, hid)], load_sems.at[2]),
        pltpu.make_async_copy(dw_hbm.at[0], dw, load_sems.at[3]),
    ]
    for load in loads:
        load.start()

    ids = ids_ref[...]
    id0, id1 = ids[:, 0:1], ids[:, 1:2]
    rw = rw_ref[...]
    lanes = lax.broadcasted_iota(jnp.int32, (tokens, 128), 1)
    hit0 = jnp.where(id0 == lanes, 1.0, 0.0).astype(F32)
    hit1 = jnp.where(id1 == lanes, 1.0, 0.0).astype(F32)
    rows = lax.broadcasted_iota(jnp.int32, (tokens, tokens), 0)
    cols = lax.broadcasted_iota(jnp.int32, (tokens, tokens), 1)
    earlier = jnp.where(rows > cols, 1.0, 0.0).astype(BF)
    counts = dot(earlier, (hit0 + hit1).astype(BF), ((1,), (0,)))
    rank0 = jnp.sum(counts * hit0, axis=1, keepdims=True)
    rank1 = jnp.sum(counts * hit1, axis=1, keepdims=True)
    slot0 = id0.astype(F32) * float(cap) + rank0
    slot1 = id1.astype(F32) * float(cap) + rank1
    places = lax.broadcasted_iota(jnp.int32, (tokens, experts * cap), 1).astype(F32)
    d0 = jnp.where(slot0 == places, 1.0, 0.0).astype(BF)
    d1 = jnp.where(slot1 == places, 1.0, 0.0).astype(BF)
    disp[...] = d0 + d1
    og = og_ref[...].astype(F32)
    sent = dot(d0, (rw[:, 0:1] * og).astype(BF), ((0,), (0,)))
    sent = sent + dot(d1, (rw[:, 1:2] * og).astype(BF), ((0,), (0,)))
    outgoing[...] = sent.astype(BF)

    greet(n_sp, me, (sib, far))
    ex = Exchange(
        n_sp, me, tp, sib, far,
        lambda k: outgoing.at[pl.ds(pl.multiple_of(k * cap, cap), cap), :],
        lambda j, s: routed.at[
            pl.ds(pl.multiple_of(s * cap, cap), cap), pl.ds(pl.multiple_of(j * chan, chan), chan)
        ],
        ex_sems,
    )
    ex.start()
    for load in loads:
        load.wait()
    tile = 256
    pre_tiles = 2 * hid // tile
    both = min(pre_tiles, n_sp - 1)

    def pre_dot(t):
        at = pl.ds(pl.multiple_of(t * tile, tile), tile)
        pre[:, at] = dot(x[...], w[:, at], ((1,), (0,)))

    @pl.loop(0, both)
    def _(t):
        ex.step(t + 1)
        pre_dot(t)

    if both < pre_tiles:
        pl.loop(both, pre_tiles)(pre_dot)
    if both < n_sp - 1:
        ex.steps(both + 1, n_sp)
    ex.finish()

    @pl.loop(0, hid // tile)
    def _(t):
        at = pl.ds(pl.multiple_of(t * tile, tile), tile)
        up_at = pl.ds(pl.multiple_of(hid + t * tile, tile), tile)
        d_hidden = dot(routed[...], dw[at, :], ((1,), (1,)))
        gate, up = pre[:, at], pre[:, up_at]
        sig = jax.nn.sigmoid(gate)
        act = gate * sig
        hidden[:, at] = (act * up).astype(BF)
        dall[:, at] = (d_hidden * up * sig * (1.0 + gate * (1.0 - sig))).astype(BF)
        dall[:, up_at] = (d_hidden * act).astype(BF)

    def back_part(block, place):
        @pl.loop(0, chan // tile)
        def _(t):
            at = pl.ds(pl.multiple_of(block * chan + t * tile, tile), tile)
            value = dot(dall[...], w[at, :], ((1,), (1,)))
            parts[place, :, pl.ds(pl.multiple_of(t * tile, tile), tile)] = value.astype(BF)

    far_sib = lax.rem(sib + n_tp // 2, n_tp)
    sib_copies = [
        remote(parts.at[2 * i], from_sib.at[i], sib_sems.at[0, i], sib_sems.at[1, i], {"tp": sib})
        for i in range(2)
    ]

    def at_rows(d):
        s = lax.rem(me + d, n_sp)
        return pl.ds(pl.multiple_of(s * cap, cap), cap)

    def far_copy(d):
        return remote(
            far_out.at[at_rows(d), :], far_in.at[at_rows(d), :],
            far_sems.at[0, lax.rem(d, n_sp)], far_sems.at[1, lax.rem(d, n_sp)], {"tp": far},
        )

    def ret_copy(d):
        mine = pl.ds(pl.multiple_of(me * cap, cap), cap)
        return remote(
            final.at[at_rows(d), :], back.at[mine, :],
            ret_sems.at[0, d], ret_sems.at[1, d], {"sp": lax.rem(me + d, n_sp)},
        )

    back_part(far_sib, 0)
    sib_copies[0].start()
    back_part(far, 1)
    sib_copies[0].wait_recv()

    @pl.loop(1, n_sp + 1)
    def _(d):
        at = at_rows(d)
        far_out[at, :] = (parts[1, at, :].astype(F32) + from_sib[0, at, :].astype(F32)).astype(BF)
        far_copy(d).start()

    back_part(sib, 2)
    sib_copies[1].start()
    back_part(tp, 3)
    sib_copies[1].wait_recv()
    total[...] = parts[3].astype(F32) + from_sib[1].astype(F32)

    @pl.loop(1, n_sp)
    def _(d):
        at = at_rows(d)
        far_copy(d).wait_recv()
        final[at, :] = (total[at, :] + far_in[at, :].astype(F32)).astype(BF)
        ret_copy(d).start()

    far_copy(n_sp).wait_recv()
    at = at_rows(0)
    back[at, :] = (total[at, :] + far_in[at, :].astype(F32)).astype(BF)

    @pl.loop(1, n_sp)
    def _(d):
        ret_copy(d).wait_recv()

    value = (og_ref[...].astype(F32) + dot(disp[...], back[...], ((1,), (0,)))).astype(BF)
    resid[...] = value
    rfull[tp] = value
    near = remote(rfull.at[tp], rfull.at[tp], gat_sems.at[0], gat_sems.at[1], {"tp": sib})
    away = remote(rfull.at[tp], rfull.at[tp], gat_sems.at[2], gat_sems.at[3], {"tp": far})
    away.start()
    near.start()
    away.wait_recv()
    hand = remote(rfull.at[far], rfull.at[far], gat_sems.at[4], gat_sems.at[5], {"tp": sib})
    hand.start()
    near.wait_recv()
    hand.wait_recv()
    share = tokens // n_tp
    piece = width // n_sp
    for k in range(n_sp):
        block, first = divmod(k * piece, chan)
        quarter[k] = rfull[
            block, pl.ds(pl.multiple_of(tp * share, share), share), first:first + piece
        ]
    near.wait_send()
    away.wait_send()
    hand.wait_send()
    for copy in sib_copies:
        copy.wait_send()

    @pl.loop(1, n_sp)
    def _(d):
        far_copy(d).wait_send()
        ret_copy(d).wait_send()

    far_copy(n_sp).wait_send()


def mixer_kernel(
    n_sp, n_tp,
    quarter, rfull, pw_hbm, og_ref, ig_ref, val_ref, conv_ref, taps_ref,
    columns, og_out, ig_out, val_out,
    pw, edge_out, edge_in, ex_sems, halo_sems, load_sem,
):
    me, tp = lax.axis_index("sp"), lax.axis_index("tp")
    sib = tp + 1 - 2 * lax.rem(tp, 2)
    far = lax.rem(tp + n_tp // 2, n_tp)
    tokens, chan = og_ref.shape
    load = pltpu.make_async_copy(pw_hbm, pw, load_sem)
    load.start()
    greet(n_sp, me, (sib, far))
    ex = Exchange(
        n_sp, me, tp, sib, far, lambda k: quarter.at[k], lambda j, s: columns.at[s, j], ex_sems
    )
    ex.start()
    load.wait()
    mix = dot(rfull[0], pw[0:chan, :], ((1,), (0,)))
    for j in range(1, n_tp):
        mix = mix + dot(rfull[j], pw[j * chan:(j + 1) * chan, :], ((1,), (0,)))
    og_out[...] = (mix * conv_ref[...].astype(F32)).astype(BF)
    grad = (mix * og_ref[...].astype(F32)).astype(BF).astype(F32)
    edge_out[0] = jnp.broadcast_to(grad[tokens - 1:tokens, :], edge_out.shape[1:])
    edge_out[1] = jnp.broadcast_to(grad[0:1, :], edge_out.shape[1:])
    sides = [lax.rem(me + 1, n_sp), lax.rem(me + n_sp - 1, n_sp)]
    halos = [
        remote(edge_out.at[i], edge_in.at[i], halo_sems.at[0, i], halo_sems.at[1, i], {"sp": sides[i]})
        for i in range(2)
    ]
    for halo in halos:
        halo.start()
    ex.steps(1, n_sp)
    for halo in halos:
        halo.wait()
    before = jnp.where(me == 0, 0.0, edge_in[0, 0:1, :])
    after = jnp.where(me == n_sp - 1, 0.0, edge_in[1, 0:1, :])
    row = lax.broadcasted_iota(jnp.int32, (tokens, chan), 0)
    prev = jnp.where(row == 0, before, pltpu.roll(grad, 1, 0))
    following = jnp.where(row == tokens - 1, after, pltpu.roll(grad, tokens - 1, 0))
    taps = taps_ref[...].astype(F32)
    value_grad = following * taps[0:1, :] + grad * taps[1:2, :] + prev * taps[2:3, :]
    ig_out[...] = (value_grad * val_ref[...].astype(F32)).astype(BF)
    val_out[...] = (value_grad * ig_ref[...].astype(F32)).astype(BF)
    ex.finish()


def in_grads(scale, x, d, gate, up):
    hid = gate.shape[-1]
    left = x[0].T
    gate[0] = (dot(left, d[:, :hid], ((1,), (0,))) * scale).astype(BF)
    up[0] = (dot(left, d[:, hid:], ((1,), (0,))) * scale).astype(BF)


def out_grads(scale, h, r, down):
    down[0] = (dot(h[...].T, r[...], ((1,), (0,))) * scale).astype(BF)


def per_device(
    out_grad, route_ids, route_weight, expert_inputs, gate_weight, up_weight, down_weight,
    out_gate, in_gate, values, conv_out, conv_taps, proj_weight,
):
    n_sp, n_tp = lax.axis_size("sp"), lax.axis_size("tp")
    tokens, chan = out_grad.shape
    local, slots, width = expert_inputs.shape
    hid = gate_weight.shape[2]
    assert local == 1 and n_tp == 4
    share, piece = tokens // n_tp, width // n_sp
    dma = pltpu.SemaphoreType.DMA
    mixed_in = (out_gate.astype(F32) * conv_out.astype(F32)).astype(BF)
    mixed_all = lax.all_gather(mixed_in, "sp", axis=0, tiled=True)

    routed, hidden, dall, resid, rfull, quarter = pl.pallas_call(
        functools.partial(expert_kernel, n_sp, n_tp, n_sp * local),
        out_shape=[
            jax.ShapeDtypeStruct((slots, width), BF),
            jax.ShapeDtypeStruct((slots, hid), BF),
            jax.ShapeDtypeStruct((slots, 2 * hid), BF),
            jax.ShapeDtypeStruct((tokens, chan), BF),
            jax.ShapeDtypeStruct((n_tp, tokens, chan), BF),
            jax.ShapeDtypeStruct((n_sp, share, piece), BF),
        ],
        in_specs=[VMEM] * 3 + [ANY] * 4,
        out_specs=[VMEM] * 6,
        scratch_shapes=[
            pltpu.VMEM((slots, width), BF),
            pltpu.VMEM((width, 2 * hid), BF),
            pltpu.VMEM((hid, width), BF),
            pltpu.VMEM((slots, 2 * hid), F32),
            pltpu.VMEM((slots, chan), BF),
            pltpu.VMEM((4, slots, chan), BF),
            pltpu.VMEM((2, slots, chan), BF),
            pltpu.VMEM((slots, chan), BF),
            pltpu.VMEM((slots, chan), BF),
            pltpu.VMEM((slots, chan), F32),
            pltpu.VMEM((slots, chan), BF),
            pltpu.VMEM((slots, chan), BF),
            pltpu.VMEM((tokens, slots), BF),
            dma((4,)), dma((8, n_sp)), dma((2, 2)), dma((2, n_sp)), dma((2, n_sp)), dma((6,)),
        ],
        compiler_params=pltpu.CompilerParams(
            collective_id=0, has_side_effects=True, vmem_limit_bytes=48 * 2**20
        ),
        name="experts",
    )(out_grad, route_ids, route_weight, expert_inputs, gate_weight, up_weight, down_weight)

    columns, out_gate_grad, in_gate_grad, values_grad = pl.pallas_call(
        functools.partial(mixer_kernel, n_sp, n_tp),
        out_shape=[
            jax.ShapeDtypeStruct((n_sp, n_tp, share, piece), BF),
            jax.ShapeDtypeStruct((tokens, chan), BF),
            jax.ShapeDtypeStruct((tokens, chan), BF),
            jax.ShapeDtypeStruct((tokens, chan), BF),
        ],
        in_specs=[VMEM, VMEM, ANY] + [VMEM] * 5,
        out_specs=[VMEM] * 4,
        scratch_shapes=[
            pltpu.VMEM(proj_weight.shape, BF),
            pltpu.VMEM((2, 8, chan), F32),
            pltpu.VMEM((2, 8, chan), F32),
            dma((8, n_sp)), dma((2, 2)), dma,
        ],
        compiler_params=pltpu.CompilerParams(
            collective_id=1, has_side_effects=True, vmem_limit_bytes=32 * 2**20
        ),
        name="mixer",
    )(quarter, rfull, proj_weight, out_gate, in_gate, values, conv_out, conv_taps)

    slot_scale = 1.0 / math.sqrt(slots)
    wide = 256
    gate_grad, up_grad = pl.pallas_call(
        functools.partial(in_grads, slot_scale),
        grid=(width // wide,),
        in_specs=[
            pl.BlockSpec((1, slots, wide), lambda i: (0, 0, i)),
            pl.BlockSpec((slots, 2 * hid), lambda i: (0, 0)),
        ],
        out_specs=[pl.BlockSpec((1, wide, hid), lambda i: (0, i, 0))] * 2,
        out_shape=[jax.ShapeDtypeStruct((1, width, hid), BF)] * 2,
        name="in_grads",
    )(expert_inputs, dall)
    down_grad = pl.pallas_call(
        functools.partial(out_grads, slot_scale),
        grid=(hid // 256,),
        in_specs=[
            pl.BlockSpec((slots, 256), lambda i: (0, i)),
            pl.BlockSpec((slots, width), lambda i: (0, 0)),
        ],
        out_specs=pl.BlockSpec((1, 256, width), lambda i: (0, i, 0)),
        out_shape=jax.ShapeDtypeStruct((1, hid, width), BF),
        name="out_grads",
    )(hidden, routed)
    proj_sum = lax.dot_general(
        columns.reshape(n_sp * tokens, piece), mixed_all,
        (((0,), (0,)), ((), ())), preferred_element_type=F32,
    )
    proj_grad = proj_sum * (1.0 / math.sqrt(tokens * n_sp))
    return (
        resid, out_gate_grad, in_gate_grad, values_grad, proj_grad, gate_grad, up_grad, down_grad,
    )


def solution(mesh):
    rows = P("sp", "tp")
    in_specs = (
        rows, P("sp", None), P("sp", None), P("sp", None, None), P("sp", None, "tp"),
        P("sp", None, "tp"), P("sp", "tp", None), rows, rows, rows, rows, P(None, "tp"), P(None, "tp"),
    )
    out_specs = (
        rows, rows, rows, rows, rows, P("sp", None, "tp"), P("sp", None, "tp"), P("sp", "tp", None),
    )
    return jax.shard_map(
        per_device, mesh=mesh, in_specs=in_specs, out_specs=out_specs, check_vma=False
    )
```

time: 200 us -> 122 us (0.61)
  Pallas kernels: 0 us -> 96.5 us
  waiting for transfers between devices: 60.4 us -> 0.02 us
  matrix products: 43.4 us -> 2.47 us
  blocking collectives: 28.2 us -> 0 us
  local copies, waits for them, and re-layouts: 27.8 us -> 6.45 us
  starting transfers between devices: 16.2 us -> 0.04 us
  other arithmetic: 8.51 us -> 1.66 us
    pallas_call x0 -> x4, Pallas kernels: none -> 96.5 us  [the longest x1 59.4 us: per_device(): pl.pallas_call(functools.partial(expert_kernel, n_sp, n_tp, n_sp * local)...]
    dot_general x12 -> x1, matrix products: 43.4 us -> 2.47 us  [per_device(): lax.dot_general(columns.reshape(n_sp * tokens, piece), mixed_all, (((0,),...]
    reduce_scatter x1 -> x0, waiting for transfers between devices: 31.1 us -> none  [expert_pass(): lax.psum_scatter(jnp.stack(partials).astype(jnp.bfloat16), 'tp', scatter_...]
    all_to_all x1 -> x0, blocking collectives: 21.7 us -> none  [expert_pass(): lax.all_to_all(outgoing, 'sp', split_axis=0, concat_axis=1, tiled=True)]
    all_gather x2 -> x1, waiting for transfers between devices: 14.8 us -> 0.01 us  [per_device(): mixed_all = lax.all_gather(mixed_in, 'sp', axis=0, tiled=True)]
    all_to_all x2 -> x0, waiting for transfers between devices: 14.4 us -> none  [the longest x1 8.71 us: expert_pass(): lax.all_to_all(summed, 'sp', split_axis=1, concat_axis=0, tiled=True)]
    unnamed x35 -> x26, local copies, waits for them, and re-layouts: 18.7 us -> 6.45 us
    all_to_all x2 -> x0, starting transfers between devices: 11.3 us -> none  [the longest x1 5.76 us: per_device(): lax.all_to_all(resid_full, 'sp', split_axis=1, concat_axis=0, tiled=True)]
  transfers between devices with their start and end apart: 7 -> 1, of which waited for: 5 -> 0; matrix products, arithmetic and copies ran while one was open for 19% -> 1% of each run, Pallas kernels for 0% -> 80%
where the time goes in v1:
time: 122 us; the launch traced here: 121 us
  Pallas kernels  96.5 us (79%)
  between operations  14.1 us (12%)
  local copies, waits for them, and re-layouts  6.45 us (5%)
  matrix products  2.47 us (2%)
  other arithmetic  1.66 us (1%)
    pallas_call x1, Pallas kernels, per_device(): pl.pallas_call(functools.partial(expert_kernel, n_sp, n_tp, n_sp * local)...  59.4 us
    pallas_call x1, Pallas kernels, per_device(): pl.pallas_call(functools.partial(mixer_kernel, n_sp, n_tp), out_shape=[ja...  23.2 us
    pallas_call x1, Pallas kernels, per_device(): pl.pallas_call(functools.partial(in_grads, slot_scale), grid=(width // wi...  8.64 us
    unnamed x26, local copies, waits for them, and re-layouts  6.45 us
    pallas_call x1, Pallas kernels, per_device(): pl.pallas_call(functools.partial(out_grads, slot_scale), grid=(hid // 256...  5.28 us
    dot_general x1, matrix products, per_device(): lax.dot_general(columns.reshape(n_sp * tokens, piece), mixed_all, (((0,),...  2.47 us
  transfers between devices with their start and end apart: 1, of which 0 were waited for; matrix products, arithmetic and copies ran while one was open for 1% of the time, Pallas kernels for 80%

profile of v1, /device:TPU:0, one launch (start us, length us, event | category | flops | bytes accessed | tf_op | source)
XLA Modules:
  0.0 121.3 jit_solution(15763925970649774249)
XLA Ops:
  7.2 0.0 all-gather.2.cloned.1.call-start
  7.2 1.7 %multiply_convert_fusion = bf16[128,512]{1,0:T(8,128)(2,1)} fusion(bf16[128,512]{1,0:T(8,128)(2,1)} %conv_ref.1, bf16[128,512]{1,0:T(8,128)(2,1)} %og_ref.3), kind=kLoop, calls=%fused_computation.1 | loop fusion | flops 262144 | bytes 393216 | tf_op jit(solution)/shard_map/convert_element_type | solution.py:362
  8.9 0.0 all-gather.2.cloned.1.call-update
  8.9 0.8 copy.21.ids_ref
  9.7 0.8 copy.22.rw_ref
  10.5 0.9 copy-done.6
  11.4 0.0 copy-start.8
  11.4 0.0 copy-start.9
  11.4 59.4 %experts.1 = (bf16[512,2048]{1,0:T(8,128)(2,1)S(1)}, bf16[512,768]{1,0:T(8,128)(2,1)S(1)}, bf16[512,1536]{1,0:T(8,128)(2,1)S(1)}, bf16[128,512]{1,0:T(8,128)(2,1...) custom-call(bf16[128,512]{1,0:T(8,128)(2,1)S(1)} %copy-done.6, s32[128,2]{1,0:T(8,128)S(1)} %copy.21.ids_ref, ...), custom_call_target="tpu_custom_call" | custom-call | tf_op jit(solution)/shard_map/experts/pallas_call | solution.py:365
  70.8 1.3 %copy-done = bf16[512,2048]{1,0:T(8,128)(2,1)} copy-done((bf16[512,2048]{1,0:T(8,128)(2,1)}, bf16[512,2048]{1,0:T(8,128)(2,1)S(1)}, u32[]{:S(2)}) %copy-start) | copy-done | bytes 2097176
  72.2 0.0 copy-done.5
  72.2 0.0 copy-done.7
  72.2 0.0 copy-done.8
  72.2 0.0 copy-done.9
  72.2 23.2 %mixer.1 = (bf16[8,4,32,256]{3,2,1,0:T(8,128)(2,1)S(1)}, bf16[128,512]{1,0:T(8,128)(2,1)S(1)}, bf16[128,512]{1,0:T(8,128)(2,1)S(1)}, bf16[128,512]{1,0:T(8,128)(2,1)S(1)}) custom-call(bf16[8,32,256]{2,1,0:T(8,128)(2,1)S(1)} %get-tuple-element.21.quarter, bf16[4,128,512]{2,1,0:T(8,128)(2,1)S(1)} %get-tuple-element.22.rfull, bf16[2048,512]{1,0:T(8,128)(2,1)S(1)} %copy-done.1, ...), custom_call_target="tpu_custom_call" | custom-call | tf_op jit(solution)/shard_map/mixer/pallas_call | solution.py:399
  95.4 0.0 copy-done.2
  95.4 0.0 copy-done.3
  95.4 8.6 %in_grads.1 = (bf16[1,2048,768]{2,1,0:T(8,128)(2,1)}, bf16[1,2048,768]{2,1,0:T(8,128)(2,1)}) custom-call(bf16[1,512,2048]{2,1,0:T(8,128)(2,1)} %x.1, bf16[512,1536]{1,0:T(8,128)(2,1)} %copy-done.2), custom_call_target="tpu_custom_call" | custom-call | tf_op jit(solution)/shard_map/in_grads/pallas_call | solution.py:423
  104.1 5.3 %out_grads.1 = bf16[1,768,2048]{2,1,0:T(8,128)(2,1)} custom-call(bf16[512,768]{1,0:T(8,128)(2,1)} %copy-done.3, bf16[512,2048]{1,0:T(8,128)(2,1)} %copy-done), custom_call_target="tpu_custom_call" | custom-call | tf_op jit(solution)/shard_map/out_grads/pallas_call | solution.py:434
  109.4 2.5 %convolution_multiply_fusion = f32[256,512]{1,0:T(8,128)} fusion(bf16[1024,256]{1,0:T(8,128)(2,1)S(1)} %bitcast.3, bf16[1024,512]{1,0:T(8,128)(2,1)} %all-gather.2.cloned.1.call-done), kind=kOutput, calls=%fused_computation | convolution fusion | flops 268566528 | bytes 2097152 | tf_op jit(solution)/shard_map/dot_general | solution.py:445
  111.8 0.7 copy.27
  112.5 0.7 copy.28
  113.1 0.7 copy.29
  113.8 0.7 copy.30
  (11 shorter events, 0.0 us)
Async XLA Ops:
  7.2 102.2 %all-gather.2.cloned.1.call-start = ((), (), s32[]{:S(2)}) async-start(), calls=%async_computation | async-start | bytes 1179648 | tf_op jit(solution)/shard_map/all_gather | solution.py:363
  10.5 0.9 copy-start.6
  11.4 60.8 %copy-start.1 = (bf16[2048,512]{1,0:T(8,128)(2,1)S(1)}, bf16[2048,512]{1,0:T(8,128)(2,1)}, u32[]{:S(2)}) copy-start(bf16[2048,512]{1,0:T(8,128)(2,1)} %pw_hbm.1) | copy-start | bytes 6291460
  11.4 60.8 %copy-start.4 = (bf16[128,512]{1,0:T(8,128)(2,1)S(1)}, bf16[128,512]{1,0:T(8,128)(2,1)}, u32[]{:S(2)}) copy-start(bf16[128,512]{1,0:T(8,128)(2,1)} %og_ref.3) | copy-start | bytes 393220
  11.4 60.8 %copy-start.5 = (bf16[128,512]{1,0:T(8,128)(2,1)S(1)}, bf16[128,512]{1,0:T(8,128)(2,1)}, u32[]{:S(2)}) copy-start(bf16[128,512]{1,0:T(8,128)(2,1)} %conv_ref.1) | copy-start | bytes 393220
  11.4 60.8 %copy-start.7 = (bf16[128,512]{1,0:T(8,128)(2,1)S(1)}, bf16[128,512]{1,0:T(8,128)(2,1)}, u32[]{:S(2)}) copy-start(bf16[128,512]{1,0:T(8,128)(2,1)} %ig_ref.1) | copy-start | bytes 393220
  11.4 60.8 %copy-start.8 = (bf16[128,512]{1,0:T(8,128)(2,1)S(1)}, bf16[128,512]{1,0:T(8,128)(2,1)}, u32[]{:S(2)}) copy-start(bf16[128,512]{1,0:T(8,128)(2,1)} %val_ref.1) | copy-start | bytes 393220
  11.4 60.8 %copy-start.9 = (bf16[3,512]{1,0:T(4,128)(2,1)S(1)}, bf16[3,512]{1,0:T(4,128)(2,1)}, u32[]{:S(2)}) copy-start(bf16[3,512]{1,0:T(4,128)(2,1)} %taps_ref.1) | copy-start | bytes 9220
  70.8 1.3 %copy-start = (bf16[512,2048]{1,0:T(8,128)(2,1)}, bf16[512,2048]{1,0:T(8,128)(2,1)S(1)}, u32[]{:S(2)}) copy-start(bf16[512,2048]{1,0:T(8,128)(2,1)S(1)} %get-tuple-element.31.r) | copy-start | bytes 6291460
  72.1 23.3 %copy-start.2 = (bf16[512,1536]{1,0:T(8,128)(2,1)}, bf16[512,1536]{1,0:T(8,128)(2,1)S(1)}, u32[]{:S(2)}) copy-start(bf16[512,1536]{1,0:T(8,128)(2,1)S(1)} %get-tuple-element.27.d) | copy-start | bytes 4718596
  72.1 23.3 %copy-start.3 = (bf16[512,768]{1,0:T(8,128)(2,1)}, bf16[512,768]{1,0:T(8,128)(2,1)S(1)}, u32[]{:S(2)}) copy-start(bf16[512,768]{1,0:T(8,128)(2,1)S(1)} %get-tuple-element.30.h) | copy-start | bytes 2359300
Sparse Core Ops, SparseCore 0:
  10.7 47.8 all-gather.1

commit v2 on v1

--- a/solution.py
+++ b/solution.py
@@ -25,7 +25,7 @@
     )
 
 
-def greet(n_sp, me, partners):
+def hail(n_sp, me, partners):
     barrier = pltpu.get_barrier_semaphore()
     for d in range(1, n_sp):
         pl.semaphore_signal(
@@ -33,7 +33,10 @@
         )
     for tp in partners:
         pl.semaphore_signal(barrier, inc=1, device_id={"tp": tp}, device_id_type=MESH)
-    pl.semaphore_wait(barrier, n_sp - 1 + len(partners))
+
+
+def met(n_sp, partners):
+    pl.semaphore_wait(pltpu.get_barrier_semaphore(), n_sp - 1 + len(partners))
 
 
 class Exchange:
@@ -74,22 +77,17 @@
         self.far_copy(0).start()
         self.sib_copy(0).start()
 
-    def step(self, d):
+    def spread(self, d):
         self.sp_copy(d).wait_recv()
         self.far_copy(d).start()
         self.sib_copy(d).start()
-        self.far_copy(d - 1).wait_recv()
-        self.hand_copy(d - 1).start()
-
-    def steps(self, first, last):
-        @pl.loop(first, last)
-        def _(d):
-            self.step(d)
+
+    def hand(self, d):
+        self.far_copy(d).wait_recv()
+        self.hand_copy(d).start()
 
     def finish(self):
         n = self.n_sp
-        self.far_copy(n - 1).wait_recv()
-        self.hand_copy(n - 1).start()
 
         @pl.loop(0, n)
         def _(d):
@@ -129,6 +127,7 @@
     for load in loads:
         load.start()
 
+    hail(n_sp, me, (sib, far))
     ids = ids_ref[...]
     id0, id1 = ids[:, 0:1], ids[:, 1:2]
     rw = rw_ref[...]
@@ -152,7 +151,7 @@
     sent = sent + dot(d1, (rw[:, 1:2] * og).astype(BF), ((0,), (0,)))
     outgoing[...] = sent.astype(BF)
 
-    greet(n_sp, me, (sib, far))
+    met(n_sp, (sib, far))
     ex = Exchange(
         n_sp, me, tp, sib, far,
         lambda k: outgoing.at[pl.ds(pl.multiple_of(k * cap, cap), cap), :],
@@ -174,13 +173,15 @@
 
     @pl.loop(0, both)
     def _(t):
-        ex.step(t + 1)
+        ex.spread(t + 1)
         pre_dot(t)
+        ex.hand(t)
 
     if both < pre_tiles:
         pl.loop(both, pre_tiles)(pre_dot)
     if both < n_sp - 1:
-        ex.steps(both + 1, n_sp)
+        pl.loop(both + 1, n_sp)(ex.spread)
+    pl.loop(both, n_sp)(ex.hand)
     ex.finish()
 
     @pl.loop(0, hid // tile)
@@ -302,7 +303,8 @@
     tokens, chan = og_ref.shape
     load = pltpu.make_async_copy(pw_hbm, pw, load_sem)
     load.start()
-    greet(n_sp, me, (sib, far))
+    hail(n_sp, me, (sib, far))
+    met(n_sp, (sib, far))
     ex = Exchange(
         n_sp, me, tp, sib, far, lambda k: quarter.at[k], lambda j, s: columns.at[s, j], ex_sems
     )
@@ -322,7 +324,8 @@
     ]
     for halo in halos:
         halo.start()
-    ex.steps(1, n_sp)
+    pl.loop(1, n_sp)(ex.spread)
+    pl.loop(0, n_sp)(ex.hand)
     for halo in halos:
         halo.wait()
     before = jnp.where(me == 0, 0.0, edge_in[0, 0:1, :])
@@ -419,7 +422,7 @@
     )(quarter, rfull, proj_weight, out_gate, in_gate, values, conv_out, conv_taps)
 
     slot_scale = 1.0 / math.sqrt(slots)
-    wide = 256
+    wide = 512
     gate_grad, up_grad = pl.pallas_call(
         functools.partial(in_grads, slot_scale),
         grid=(width // wide,),

time: 122 us -> 110 us (0.902)
  Pallas kernels: 96.5 us -> 85 us
    pallas_call x1, Pallas kernels: 23.2 us -> 14.1 us  [per_device(): pl.pallas_call(functools.partial(mixer_kernel, n_sp, n_tp), out_shape=[ja...]
    pallas_call x1, Pallas kernels: 8.64 us -> 6.92 us  [per_device(): pl.pallas_call(functools.partial(in_grads, slot_scale), grid=(width // wi...]
  transfers between devices with their start and end apart: 1 -> 1, of which waited for: 0 -> 0; matrix products, arithmetic and copies ran while one was open for 1% -> 1% of each run, Pallas kernels for 80% -> 77%
where the time goes in v2:
time: 110 us
  Pallas kernels  85 us (77%)
  between operations  14.1 us (13%)
  local copies, waits for them, and re-layouts  6.45 us (6%)
  matrix products  2.48 us (2%)
  other arithmetic  1.66 us (2%)
    pallas_call x1, Pallas kernels, per_device(): pl.pallas_call(functools.partial(expert_kernel, n_sp, n_tp, n_sp * local)...  58.7 us
    pallas_call x1, Pallas kernels, per_device(): pl.pallas_call(functools.partial(mixer_kernel, n_sp, n_tp), out_shape=[ja...  14.1 us
    pallas_call x1, Pallas kernels, per_device(): pl.pallas_call(functools.partial(in_grads, slot_scale), grid=(width // wi...  6.92 us
    unnamed x26, local copies, waits for them, and re-layouts  6.45 us
    pallas_call x1, Pallas kernels, per_device(): pl.pallas_call(functools.partial(out_grads, slot_scale), grid=(hid // 256...  5.28 us
    dot_general x1, matrix products, per_device(): lax.dot_general(columns.reshape(n_sp * tokens, piece), mixed_all, (((0,),...  2.48 us
  transfers between devices with their start and end apart: 1, of which 0 were waited for; matrix products, arithmetic and copies ran while one was open for 1% of the time, Pallas kernels for 77%

profile of v2, /device:TPU:0, one launch (start us, length us, event | category | flops | bytes accessed | tf_op | source)
XLA Modules:
  0.0 109.8 jit_solution(9440159171710733266)
XLA Ops:
  7.2 0.0 all-gather.2.cloned.1.call-start
  7.2 1.7 %multiply_convert_fusion = bf16[128,512]{1,0:T(8,128)(2,1)} fusion(bf16[128,512]{1,0:T(8,128)(2,1)} %conv_ref.1, bf16[128,512]{1,0:T(8,128)(2,1)} %og_ref.3), kind=kLoop, calls=%fused_computation.1 | loop fusion | flops 262144 | bytes 393216 | tf_op jit(solution)/shard_map/convert_element_type | solution.py:365
  8.9 0.0 all-gather.2.cloned.1.call-update
  8.9 0.8 copy.21.ids_ref
  9.7 0.8 copy.22.rw_ref
  10.5 0.9 copy-done.6
  11.4 0.0 copy-start.8
  11.4 0.0 copy-start.9
  11.4 58.7 %experts.1 = (bf16[512,2048]{1,0:T(8,128)(2,1)S(1)}, bf16[512,768]{1,0:T(8,128)(2,1)S(1)}, bf16[512,1536]{1,0:T(8,128)(2,1)S(1)}, bf16[128,512]{1,0:T(8,128)(2,1...) custom-call(bf16[128,512]{1,0:T(8,128)(2,1)S(1)} %copy-done.6, s32[128,2]{1,0:T(8,128)S(1)} %copy.21.ids_ref, ...), custom_call_target="tpu_custom_call" | custom-call | tf_op jit(solution)/shard_map/experts/pallas_call | solution.py:368
  70.1 0.0 copy-start
  70.2 1.3 %copy-done = bf16[512,2048]{1,0:T(8,128)(2,1)} copy-done((bf16[512,2048]{1,0:T(8,128)(2,1)}, bf16[512,2048]{1,0:T(8,128)(2,1)S(1)}, u32[]{:S(2)}) %copy-start) | copy-done | bytes 2097176
  71.5 0.0 copy-done.1
  71.5 0.0 copy-done.5
  71.5 0.0 copy-done.7
  71.5 0.0 copy-done.8
  71.5 0.0 copy-done.9
  71.5 14.1 %mixer.1 = (bf16[8,4,32,256]{3,2,1,0:T(8,128)(2,1)S(1)}, bf16[128,512]{1,0:T(8,128)(2,1)S(1)}, bf16[128,512]{1,0:T(8,128)(2,1)S(1)}, bf16[128,512]{1,0:T(8,128)(2,1)S(1)}) custom-call(bf16[8,32,256]{2,1,0:T(8,128)(2,1)S(1)} %get-tuple-element.21.quarter, bf16[4,128,512]{2,1,0:T(8,128)(2,1)S(1)} %get-tuple-element.22.rfull, bf16[2048,512]{1,0:T(8,128)(2,1)S(1)} %copy-done.1, ...), custom_call_target="tpu_custom_call" | custom-call | tf_op jit(solution)/shard_map/mixer/pallas_call | solution.py:402
  85.7 6.9 %in_grads.1 = (bf16[1,2048,768]{2,1,0:T(8,128)(2,1)}, bf16[1,2048,768]{2,1,0:T(8,128)(2,1)}) custom-call(bf16[1,512,2048]{2,1,0:T(8,128)(2,1)} %x.1, bf16[512,1536]{1,0:T(8,128)(2,1)} %copy-done.2), custom_call_target="tpu_custom_call" | custom-call | tf_op jit(solution)/shard_map/in_grads/pallas_call | solution.py:426
  92.6 5.3 %out_grads.1 = bf16[1,768,2048]{2,1,0:T(8,128)(2,1)} custom-call(bf16[512,768]{1,0:T(8,128)(2,1)} %copy-done.3, bf16[512,2048]{1,0:T(8,128)(2,1)} %copy-done), custom_call_target="tpu_custom_call" | custom-call | tf_op jit(solution)/shard_map/out_grads/pallas_call | solution.py:437
  97.9 2.5 %convolution_multiply_fusion = f32[256,512]{1,0:T(8,128)} fusion(bf16[1024,256]{1,0:T(8,128)(2,1)S(1)} %bitcast.3, bf16[1024,512]{1,0:T(8,128)(2,1)} %all-gather.2.cloned.1.call-done), kind=kOutput, calls=%fused_computation | convolution fusion | flops 268566528 | bytes 2097152 | tf_op jit(solution)/shard_map/dot_general | solution.py:448
  100.4 0.7 copy.27
  101.0 0.7 copy.28
  101.7 0.7 copy.29
  102.3 0.7 copy.30
  (11 shorter events, 0.0 us)
Async XLA Ops:
  7.2 90.7 %all-gather.2.cloned.1.call-start = ((), (), s32[]{:S(2)}) async-start(), calls=%async_computation | async-start | bytes 1179648 | tf_op jit(solution)/shard_map/all_gather | solution.py:366
  10.5 0.9 copy-start.6
  11.4 60.1 %copy-start.1 = (bf16[2048,512]{1,0:T(8,128)(2,1)S(1)}, bf16[2048,512]{1,0:T(8,128)(2,1)}, u32[]{:S(2)}) copy-start(bf16[2048,512]{1,0:T(8,128)(2,1)} %pw_hbm.1) | copy-start | bytes 6291460
  11.4 60.1 %copy-start.4 = (bf16[128,512]{1,0:T(8,128)(2,1)S(1)}, bf16[128,512]{1,0:T(8,128)(2,1)}, u32[]{:S(2)}) copy-start(bf16[128,512]{1,0:T(8,128)(2,1)} %og_ref.3) | copy-start | bytes 393220
  11.4 60.1 %copy-start.5 = (bf16[128,512]{1,0:T(8,128)(2,1)S(1)}, bf16[128,512]{1,0:T(8,128)(2,1)}, u32[]{:S(2)}) copy-start(bf16[128,512]{1,0:T(8,128)(2,1)} %conv_ref.1) | copy-start | bytes 393220
  11.4 60.1 %copy-start.7 = (bf16[128,512]{1,0:T(8,128)(2,1)S(1)}, bf16[128,512]{1,0:T(8,128)(2,1)}, u32[]{:S(2)}) copy-start(bf16[128,512]{1,0:T(8,128)(2,1)} %ig_ref.1) | copy-start | bytes 393220
  11.4 60.1 %copy-start.8 = (bf16[128,512]{1,0:T(8,128)(2,1)S(1)}, bf16[128,512]{1,0:T(8,128)(2,1)}, u32[]{:S(2)}) copy-start(bf16[128,512]{1,0:T(8,128)(2,1)} %val_ref.1) | copy-start | bytes 393220
  11.4 60.1 %copy-start.9 = (bf16[3,512]{1,0:T(4,128)(2,1)S(1)}, bf16[3,512]{1,0:T(4,128)(2,1)}, u32[]{:S(2)}) copy-start(bf16[3,512]{1,0:T(4,128)(2,1)} %taps_ref.1) | copy-start | bytes 9220
  70.1 1.3 %copy-start = (bf16[512,2048]{1,0:T(8,128)(2,1)}, bf16[512,2048]{1,0:T(8,128)(2,1)S(1)}, u32[]{:S(2)}) copy-start(bf16[512,2048]{1,0:T(8,128)(2,1)S(1)} %get-tuple-element.31.r) | copy-start | bytes 6291460
  71.5 14.2 %copy-start.2 = (bf16[512,1536]{1,0:T(8,128)(2,1)}, bf16[512,1536]{1,0:T(8,128)(2,1)S(1)}, u32[]{:S(2)}) copy-start(bf16[512,1536]{1,0:T(8,128)(2,1)S(1)} %get-tuple-element.27.d) | copy-start | bytes 4718596
  71.5 14.2 %copy-start.3 = (bf16[512,768]{1,0:T(8,128)(2,1)}, bf16[512,768]{1,0:T(8,128)(2,1)S(1)}, u32[]{:S(2)}) copy-start(bf16[512,768]{1,0:T(8,128)(2,1)S(1)} %get-tuple-element.30.h) | copy-start | bytes 2359300
Sparse Core Ops, SparseCore 0:
  10.7 53.6 all-gather.1
